TPU v7x, 512 devices: a 4x2x32 block of a 4x8x32 slice. The times are simulated.
512 devices in a mesh: grp: 2 (over y), fs: 32 (over z), tp: 8 (over x, core).
Axes of the slice: x: 4, y: 2, z: 32, core: 2. Of those that a mesh axis runs over, the one named last changes fastest.
The devices are a block of a 4x8x32 slice.
Arguments:
- tokens: bfloat16 [20480, 2048], P(('grp', 'fs', 'tp')), parts along dimension 0, may hold values from -6 to 6
- mix_gain: bfloat16 [2048], replicated, may hold values from 0.099609375 to 1.8984375
- val_weight: bfloat16 [2048, 1024], P('fs', 'tp'), may hold values from -4 to 4
- gate_weight: bfloat16 [2048, 1024], P('fs', 'tp'), may hold values from -0.125 to 0.125
- conv_taps: bfloat16 [31, 1024], replicated, may hold values from -1 to 1
- chan_gain: bfloat16 [1024], replicated, may hold values from 0.099609375 to 1.8984375
- out_weight: bfloat16 [1024, 2048], P('tp', 'fs'), may hold values from -0.1875 to 0.1875
- mix_post_gain: bfloat16 [2048], replicated, may hold values from 0.099609375 to 1.8984375
- ffn_gain: bfloat16 [2048], replicated, may hold values from 0.099609375 to 1.8984375
- up_gate_weight: bfloat16 [2048, 5120], P('fs', 'tp'), may hold values from -0.125 to 0.125
- up_val_weight: bfloat16 [2048, 5120], P('fs', 'tp'), may hold values from -0.125 to 0.125
- ffn_taps: bfloat16 [2, 3, 5120], replicated, may hold values from -3.5 to 3.5
- down_weight: bfloat16 [5120, 2048], P('tp', 'fs'), may hold values from -0.078125 to 0.078125
- ffn_post_gain: bfloat16 [2048], replicated, may hold values from 0.099609375 to 1.8984375
Outputs:
- layer_out: bfloat16 [20480, 2048], P(('grp', 'fs', 'tp')), parts along dimension 0
There are 2 independent parts, one for each index of `grp`. A program takes and returns all parts, laid end to end along the dimension named above; an argument that names none is the same for every part. Nothing has to cross between parts.
All inputs are finite; a program needn't handle non-finite values.
Results may differ from a plain program's by a relative error of at most 0.019.
Values may be sent and summed in bfloat16 or wider, within the bound.
A program may use at most 64 MiB of HBM per device.

v0:
```python
import jax
import jax.numpy as jnp
from jax import lax
from jax.sharding import PartitionSpec as P

LEN = 64
norm_epsilon = 1e-06
chan_epsilon = 1e-05


def from_everyone(array, axis):
    copies = jnp.broadcast_to(array, (lax.axis_size(axis), *array.shape))
    return lax.all_to_all(copies, axis, split_axis=0, concat_axis=0, tiled=True)


def laid_out(blocks, dim):
    blocks = jnp.moveaxis(blocks, 0, dim)
    lengths = blocks.shape
    return blocks.reshape(*lengths[:dim], lengths[dim] * lengths[dim + 1], *lengths[dim + 2 :])


def gathered_copies(array, axis, dim):
    blocks = from_everyone(array, axis)
    return laid_out(blocks, dim)


def sent_together(arrays, axis, dim, along):
    ends, at = ([], 0)
    for a in arrays[:-1]:
        at += a.shape[along]
        ends.append(at)
    both = jnp.concatenate(arrays, axis=along)
    return tuple(jnp.split(lax.all_gather(both, axis, axis=dim, tiled=True), ends, axis=along))


def over_copies(array, axis):
    return from_everyone(array, axis).sum(axis=0)


def together(arrays, axis):
    ends = [0]
    for a in arrays:
        ends.append(ends[-1] + a.size)
    total = over_copies(jnp.concatenate([a.ravel() for a in arrays]), axis)
    return tuple((total[b:e].reshape(a.shape) for a, b, e in zip(arrays, ends, ends[1:])))


def in_blocks(array, dim, length):
    lengths = array.shape
    blocks = array.reshape(*lengths[:dim], length, lengths[dim] // length, *lengths[dim + 1 :])
    return jnp.moveaxis(blocks, dim, 0)


def summed_on_arrival(array, axis, dim):
    blocks = in_blocks(array, dim, lax.axis_size(axis))
    arrived = lax.all_to_all(blocks, axis, split_axis=0, concat_axis=0, tiled=True)
    return arrived.astype(jnp.float32).sum(axis=0)


def rms_scale(values, gain):
    inverse = lax.rsqrt(jnp.mean(values * values, axis=-1, keepdims=True) + norm_epsilon)
    return values * inverse * gain.astype(jnp.float32)


def depthwise(signal, tap_table):
    taps_count = tap_table.shape[0]
    channels = signal.shape[1]
    shaped = signal.astype(jnp.float32).reshape(signal.shape[0] // LEN, LEN, channels)
    padded = jnp.pad(shaped, ((0, 0), (taps_count - 1, 0), (0, 0)))
    tap_values = tap_table.astype(jnp.float32)
    result = jnp.zeros(shaped.shape, jnp.float32)
    for offset in range(taps_count):
        result = result + padded[:, offset : offset + LEN, :] * tap_values[offset]
    return result.reshape(signal.shape[0], channels)


def make_adder(left, pieces):
    first = jnp.dot(left, pieces[0], preferred_element_type=jnp.float32)
    second = jnp.dot(left, pieces[1], preferred_element_type=jnp.float32)
    return (first, second)


def make_rows_product(left, weight):
    return jnp.dot(left, weight, preferred_element_type=jnp.float32)


def shards(
    tokens,
    mix_gain,
    val_weight,
    gate_weight,
    conv_taps,
    chan_gain,
    out_weight,
    mix_post_gain,
    ffn_gain,
    up_gate_weight,
    up_val_weight,
    ffn_taps,
    down_weight,
    ffn_post_gain,
):
    member = lax.axis_index("tp")
    normed_own = rms_scale(tokens.astype(jnp.float32), mix_gain).astype(jnp.bfloat16)
    normed = gathered_copies(normed_own, "tp", 0)
    local_ch = val_weight.shape[1]
    values, gate_sums = make_adder(normed, sent_together((val_weight, gate_weight), "fs", 0, 1))
    glu_out = (values * jax.nn.sigmoid(gate_sums)).astype(jnp.bfloat16)
    own_taps = lax.dynamic_slice_in_dim(conv_taps, member * local_ch, local_ch, 1)
    conv_out = depthwise(glu_out, own_taps)
    totals, squares = together(
        (jnp.sum(conv_out, axis=1), jnp.sum(conv_out * conv_out, axis=1)), "tp"
    )
    all_channels = chan_gain.shape[0]
    chan_mean = totals[:, None] / all_channels
    chan_var = squares[:, None] / all_channels - chan_mean * chan_mean
    own_gain = lax.dynamic_slice_in_dim(chan_gain, member * local_ch, local_ch, 0).astype(
        jnp.float32
    )
    activated = jax.nn.silu((conv_out - chan_mean) * lax.rsqrt(chan_var + chan_epsilon) * own_gain)
    activated = activated.astype(jnp.bfloat16)
    out_full = lax.all_gather(out_weight, "fs", axis=1, tiled=True)
    mixed_sum = summed_on_arrival(
        make_rows_product(activated, out_full).astype(jnp.bfloat16), "tp", 0
    )
    residual = (tokens.astype(jnp.float32) + rms_scale(mixed_sum, mix_post_gain)).astype(
        jnp.bfloat16
    )
    normed_share = rms_scale(residual.astype(jnp.float32), ffn_gain).astype(jnp.bfloat16)
    normed_ffn = gathered_copies(normed_share, "tp", 0)
    local_ff = up_gate_weight.shape[1]
    own_ffn_taps = lax.dynamic_slice_in_dim(ffn_taps, member * local_ff, local_ff, 2)
    gate_full, val_full = sent_together((up_gate_weight, up_val_weight), "fs", 0, 1)
    up_gate = jnp.dot(normed_ffn, gate_full, preferred_element_type=jnp.float32).astype(
        jnp.bfloat16
    )
    up_val = jnp.dot(normed_ffn, val_full, preferred_element_type=jnp.float32).astype(jnp.bfloat16)
    gate_conv = depthwise(up_gate, own_ffn_taps[0])
    val_conv = depthwise(up_val, own_ffn_taps[1])
    hidden = (jax.nn.gelu(gate_conv, approximate=True) * val_conv).astype(jnp.bfloat16)
    down_full = lax.all_gather(down_weight, "fs", axis=1, tiled=True)
    ffn_sum = summed_on_arrival(make_rows_product(hidden, down_full).astype(jnp.bfloat16), "tp", 0)
    return (residual.astype(jnp.float32) + rms_scale(ffn_sum, ffn_post_gain)).astype(jnp.bfloat16)


def solution(mesh):
    return jax.shard_map(
        shards,
        mesh=mesh,
        in_specs=(
            P(("grp", "fs", "tp"), None),
            P(),
            P("fs", "tp"),
            P("fs", "tp"),
            P(),
            P(),
            P("tp", "fs"),
            P(),
            P(),
            P("fs", "tp"),
            P("fs", "tp"),
            P(),
            P("tp", "fs"),
            P(),
        ),
        out_specs=P(("grp", "fs", "tp"), None),
        check_vma=False,
    )
```

profile of v0, /device:TPU:33, one launch (start us, length us, event | category | flops | bytes accessed | tf_op | source)
XLA Modules:
  0.0 472.4 jit_solution(905065115232511449)
XLA Ops:
  6.5 0.0 all-gather.4.cloned.1.call-start
  6.6 1.3 pad_maximum_fusion.1
  7.9 0.1 all-gather.4.cloned.1.call-update
  8.0 0.1 all-gather.6.cloned.1.call-start
  8.0 1.6 pad_maximum_fusion
  9.6 0.1 all-gather.6.cloned.1.call-update
  9.7 0.7 convert_element_type.82
  10.4 1.1 fusion.33
  11.5 1.0 fusion.35
  12.5 1.3 broadcast_in_dim.6
  13.7 0.0 copy-start.2
  13.7 45.0 %all-to-all-start = ((bf16[8,40,2048]{2,1,0:T(8,128)(2,1)}), bf16[8,40,2048]{2,1,0:T(8,128)(2,1)S(1)}, u32[]{:S(2)}, u32[]{:S(2)}) async-start(bf16[8,40,2048]{2,1,0:T(8,128)(2,1)} %broadcast_in_dim.6), calls=%async_computation | async-start | bytes 2621440 | tf_op jit(solution)/shard_map/all_to_all | solution.py:13
  58.8 0.7 dynamic-slice_convert_fusion
  59.5 0.0 copy-done.2
  59.5 46.8 %all_gather.13 = bf16[128,2048]{0,1:T(8,128)(2,1)S(1)} all-gather(bf16[128,64]{0,1:T(8,128)(2,1)S(1)} %copy-done.2), channel_id=1, replica_groups=mesh['grp'=2,'fs'=32,'tp'=8] {'fs'}, dimensions={1}, use_global_device_ids=true | all-gather | bytes 540672 | tf_op jit(solution)/shard_map/all_gather | solution.py:122
  106.3 0.0 all-to-all-done
  106.3 43.0 %all-gather.4.cloned.1.call-done = bf16[2048,256]{1,0:T(8,128)(2,1)} async-done(((bf16[64,256]{1,0:T(8,128)(2,1)}), bf16[2048,256]{1,0:T(8,128)(2,1)}) %all-gather.4.cloned.1.call-update) | async-done | bytes 1048592 | tf_op jit(solution)/shard_map/all_gather | solution.py:33
  149.3 0.0 copy-start.1
  149.3 1.6 fusion.12
  151.0 0.0 copy-done.1
  151.0 0.5 fusion.13
  151.5 0.6 fusion.103
  152.2 0.1 reduce_sum.87
  152.2 0.1 reduce_sum.89
  152.3 0.1 pad_maximum_fusion.2
  152.4 0.6 broadcast_in_dim.7
  153.0 25.4 %all-to-all-start.1 = ((f32[8,1,640]{2,1,0:T(1,128)}), f32[8,1,640]{2,1,0:T(1,128)S(1)}, u32[]{:S(2)}, u32[]{:S(2)}) async-start(f32[8,1,640]{2,1,0:T(1,128)} %broadcast_in_dim.7), calls=%async_computation.1 | async-start | bytes 40960 | tf_op jit(solution)/shard_map/all_to_all | solution.py:13
  178.4 0.8 dynamic-slice_convert_fusion.3
  179.2 3.9 all-to-all-done.1
  183.1 0.1 slice_multiply_fusion
  183.2 0.2 multiply_convert_fusion
  183.4 1.7 convolution_convert_fusion
  185.1 4.3 all-to-all-start.2
  189.4 0.0 all-gather.8.cloned.1.call-start
  189.4 0.7 all-gather.8.cloned.1.call-update
  190.2 0.0 copy-done.3
  190.2 0.0 copy-done.4
  190.2 17.1 %all-to-all-done.2 = bf16[8,40,2048]{2,1,0:T(8,128)(2,1)S(1)} async-done(((bf16[8,40,2048]{2,1,0:T(8,128)(2,1)}), bf16[8,40,2048]{2,1,0:T(8,128)(2,1)S(1)}, u32[]{:S(2)}, u32[]{:S(2)}) %all-to-all-start.2) | async-done | bytes 1310752 | tf_op jit(solution)/shard_map/all_to_all | solution.py:56
  207.3 0.2 convert_reduce_fusion.1
  207.5 0.1 multiply_reduce_fusion.1
  207.6 0.0 copy-done
  207.6 0.2 fusion.37
  207.9 0.1 fusion.39
  208.0 1.3 broadcast_in_dim.8
  209.3 4.4 all-to-all-start.3
  213.8 0.9 dynamic-slice_convert_fusion.2
  214.7 17.0 %all-to-all-done.3 = bf16[8,40,2048]{2,1,0:T(8,128)(2,1)S(1)} async-done(((bf16[8,40,2048]{2,1,0:T(8,128)(2,1)}), bf16[8,40,2048]{2,1,0:T(8,128)(2,1)S(1)}, u32[]{:S(2)}, u32[]{:S(2)}) %all-to-all-start.3) | async-done | bytes 1310752 | tf_op jit(solution)/shard_map/all_to_all | solution.py:13
  231.6 55.6 %all-gather.6.cloned.1.call-done = bf16[2048,1280]{1,0:T(8,128)(2,1)} async-done(((bf16[64,1280]{1,0:T(8,128)(2,1)}), bf16[2048,1280]{1,0:T(8,128)(2,1)}) %all-gather.6.cloned.1.call-update) | async-done | bytes 5242896 | tf_op jit(solution)/shard_map/all_gather | solution.py:33
  287.2 3.1 fusion.4
  290.3 0.1 convert.4
  290.4 0.1 copy-done.6
  290.5 1.2 fusion.7
  291.7 0.1 convert.5
  291.7 0.2 fusion.16
  292.0 0.2 fusion.20
  292.2 0.3 fusion.30
  292.5 124.9 %all-gather.8.cloned.1.call-done = bf16[640,2048]{0,1:T(8,128)(2,1)} async-done(((bf16[640,64]{0,1:T(8,128)(2,1)}), bf16[640,2048]{0,1:T(8,128)(2,1)}) %all-gather.8.cloned.1.call-update) | async-done | bytes 2621456 | tf_op jit(solution)/shard_map/all_gather | solution.py:141
  417.5 4.0 convolution_convert_fusion.1
  421.5 25.5 %all-to-all-start.4 = ((bf16[8,40,2048]{2,1,0:T(8,128)(2,1)}), bf16[8,40,2048]{2,1,0:T(8,128)(2,1)S(1)}, u32[]{:S(2)}, u32[]{:S(2)}) async-start(bf16[8,40,2048]{2,1,0:T(8,128)(2,1)} %bitcast.43), calls=%async_computation.4 | async-start | bytes 2621440 | tf_op jit(solution)/shard_map/all_to_all | solution.py:56
  447.0 0.0 copy-done.5
  447.0 17.8 %all-to-all-done.4 = bf16[8,40,2048]{2,1,0:T(8,128)(2,1)S(1)} async-done(((bf16[8,40,2048]{2,1,0:T(8,128)(2,1)}), bf16[8,40,2048]{2,1,0:T(8,128)(2,1)S(1)}, u32[]{:S(2)}, u32[]{:S(2)}) %all-to-all-start.4) | async-done | bytes 1310752 | tf_op jit(solution)/shard_map/all_to_all | solution.py:56
  464.8 0.2 convert_reduce_fusion
  465.0 0.1 multiply_reduce_fusion
  465.1 0.8 fusion.40
  (17 shorter events, 0.2 us)
Async XLA Ops:
  6.5 142.8 %all-gather.4.cloned.1.call-start = ((), (), s32[]{:S(2)}) async-start(), calls=%async_computation.5 | async-start | bytes 1081344 | tf_op jit(solution)/shard_map/all_gather | solution.py:33
  8.0 279.3 %all-gather.6.cloned.1.call-start = ((), (), s32[]{:S(2)}) async-start(), calls=%async_computation.6 | async-start | bytes 5406720 | tf_op jit(solution)/shard_map/all_gather | solution.py:33
  13.7 45.8 %copy-start.2 = (bf16[128,64]{0,1:T(8,128)(2,1)S(1)}, bf16[128,64]{0,1:T(8,128)(2,1)}, u32[]{:S(2)}) copy-start(bf16[128,64]{0,1:T(8,128)(2,1)} %param.20) | copy-start | bytes 49156
  13.7 92.6 %all-to-all-start = ((bf16[8,40,2048]{2,1,0:T(8,128)(2,1)}), bf16[8,40,2048]{2,1,0:T(8,128)(2,1)S(1)}, u32[]{:S(2)}, u32[]{:S(2)}) async-start(bf16[8,40,2048]{2,1,0:T(8,128)(2,1)} %broadcast_in_dim.6), calls=%async_computation | async-start | bytes 2621440 | tf_op jit(solution)/shard_map/all_to_all | solution.py:13
  149.3 1.7 copy-start.1
  153.0 30.1 %all-to-all-start.1 = ((f32[8,1,640]{2,1,0:T(1,128)}), f32[8,1,640]{2,1,0:T(1,128)S(1)}, u32[]{:S(2)}, u32[]{:S(2)}) async-start(f32[8,1,640]{2,1,0:T(1,128)} %broadcast_in_dim.7), calls=%async_computation.1 | async-start | bytes 40960 | tf_op jit(solution)/shard_map/all_to_all | solution.py:13
  185.1 5.1 %copy-start.3 = (bf16[2048]{0:T(1024)(128)(2,1)S(1)}, bf16[2048]{0:T(1024)(128)(2,1)}, u32[]{:S(2)}) copy-start(bf16[2048]{0:T(1024)(128)(2,1)} %param.21) | copy-start | bytes 12292
  185.1 5.1 %copy-start.4 = (bf16[2048]{0:T(1024)(128)(2,1)S(1)}, bf16[2048]{0:T(1024)(128)(2,1)}, u32[]{:S(2)}) copy-start(bf16[2048]{0:T(1024)(128)(2,1)} %param.22) | copy-start | bytes 12292
  185.1 22.2 %all-to-all-start.2 = ((bf16[8,40,2048]{2,1,0:T(8,128)(2,1)}), bf16[8,40,2048]{2,1,0:T(8,128)(2,1)S(1)}, u32[]{:S(2)}, u32[]{:S(2)}) async-start(bf16[8,40,2048]{2,1,0:T(8,128)(2,1)} %bitcast.35), calls=%async_computation.2 | async-start | bytes 2621440 | tf_op jit(solution)/shard_map/all_to_all | solution.py:56
  189.4 18.2 %copy-start = (bf16[40,2048]{1,0:T(8,128)(2,1)S(1)}, bf16[40,2048]{1,0:T(8,128)(2,1)}, u32[]{:S(2)}) copy-start(bf16[40,2048]{1,0:T(8,128)(2,1)} %param.14) | copy-start | bytes 491524
  189.4 228.1 %all-gather.8.cloned.1.call-start = ((), (), s32[]{:S(2)}) async-start(), calls=%async_computation.7 | async-start | bytes 2703360 | tf_op jit(solution)/shard_map/all_gather | solution.py:141
  209.3 22.3 %all-to-all-start.3 = ((bf16[8,40,2048]{2,1,0:T(8,128)(2,1)}), bf16[8,40,2048]{2,1,0:T(8,128)(2,1)S(1)}, u32[]{:S(2)}, u32[]{:S(2)}) async-start(bf16[8,40,2048]{2,1,0:T(8,128)(2,1)} %broadcast_in_dim.8), calls=%async_computation.3 | async-start | bytes 2621440 | tf_op jit(solution)/shard_map/all_to_all | solution.py:13
  287.2 3.3 copy-start.6
  421.5 25.5 %copy-start.5 = (bf16[2048]{0:T(1024)(128)(2,1)S(1)}, bf16[2048]{0:T(1024)(128)(2,1)}, u32[]{:S(2)}) copy-start(bf16[2048]{0:T(1024)(128)(2,1)} %param.27) | copy-start | bytes 12292
  421.5 43.3 %all-to-all-start.4 = ((bf16[8,40,2048]{2,1,0:T(8,128)(2,1)}), bf16[8,40,2048]{2,1,0:T(8,128)(2,1)S(1)}, u32[]{:S(2)}, u32[]{:S(2)}) async-start(bf16[8,40,2048]{2,1,0:T(8,128)(2,1)} %bitcast.43), calls=%async_computation.4 | async-start | bytes 2621440 | tf_op jit(solution)/shard_map/all_to_all | solution.py:56
Sparse Core Ops, SparseCore 0:
  9.4 139.8 all-gather.3
  151.4 135.7 all-gather.5
  289.3 128.1 all-gather.7
where the time goes:
time: 473 us; the launch traced here: 472 us
  waiting for transfers between devices  280 us (59%)
  starting transfers between devices  105 us (22%)
  blocking collectives  46.8 us (10%)
  between operations  13.3 us (3%)
  matrix products  12.1 us (3%)
  other arithmetic  11.8 us (2%)
    all_gather x1, waiting for transfers between devices, shards(): down_full = lax.all_gather(down_weight, 'fs', axis=1, tiled=True)  125 us
    all_gather x2, waiting for transfers between devices, sent_together(): lax.all_gather(both, axis, axis=dim, tiled=True)  98.6 us
    all_to_all x3, starting transfers between devices, from_everyone(): return lax.all_to_all(copies, axis, split_axis=0, concat_axis=0, tiled=True)  74.9 us
    all_gather x1, blocking collectives, shards(): out_full = lax.all_gather(out_weight, 'fs', axis=1, tiled=True)  46.8 us
    all_to_all x2, waiting for transfers between devices, summed_on_arrival(): lax.all_to_all(blocks, axis, split_axis=0, concat_axis=0, tiled=True)  34.8 us
    all_to_all x2, starting transfers between devices, summed_on_arrival(): lax.all_to_all(blocks, axis, split_axis=0, concat_axis=0, tiled=True)  29.8 us
    all_to_all x3, waiting for transfers between devices, from_everyone(): return lax.all_to_all(copies, axis, split_axis=0, concat_axis=0, tiled=True)  20.9 us
  transfers between devices with their start and end apart: 8, of which 7 were waited for; matrix products, arithmetic and copies ran while one was open for 4% of the time, Pallas kernels for 0%

commit v1 on v0

--- a/solution.py
+++ b/solution.py
@@ -138,7 +138,8 @@
     gate_conv = depthwise(up_gate, own_ffn_taps[0])
     val_conv = depthwise(up_val, own_ffn_taps[1])
     hidden = (jax.nn.gelu(gate_conv, approximate=True) * val_conv).astype(jnp.bfloat16)
-    down_full = lax.all_gather(down_weight, "fs", axis=1, tiled=True)
+    copies_2 = jnp.concatenate([down_weight] * lax.axis_size("fs"), axis=1)
+    down_full = lax.all_to_all(copies_2, "fs", 1, 1, tiled=True)
     ffn_sum = summed_on_arrival(make_rows_product(hidden, down_full).astype(jnp.bfloat16), "tp", 0)
     return (residual.astype(jnp.float32) + rms_scale(ffn_sum, ffn_post_gain)).astype(jnp.bfloat16)
 

time: 473 us -> 604 us (1.28)
  waiting for transfers between devices: 280 us -> 386 us
  local copies, waits for them, and re-layouts: 3.54 us -> 25.5 us
    all_gather x2, waiting for transfers between devices: 98.6 us -> 343 us  [sent_together(): lax.all_gather(both, axis, axis=dim, tiled=True)]
    all_gather x1 -> x0, waiting for transfers between devices: 125 us -> none  [shards(): down_full = lax.all_gather(down_weight, 'fs', axis=1, tiled=True)]
    unnamed x14 -> x55, local copies, waits for them, and re-layouts: 0.14 us -> 21.6 us
    all_to_all x0 -> x1, starting transfers between devices: none -> 13.1 us  [shards(): down_full = lax.all_to_all(copies_2, 'fs', 1, 1, tiled=True)]
    all_to_all x2, starting transfers between devices: 29.8 us -> 20 us  [summed_on_arrival(): lax.all_to_all(blocks, axis, split_axis=0, concat_axis=0, tiled=True)]
    all_to_all x2, waiting for transfers between devices: 34.8 us -> 28.7 us  [summed_on_arrival(): lax.all_to_all(blocks, axis, split_axis=0, concat_axis=0, tiled=True)]
    all_to_all x3, waiting for transfers between devices: 20.9 us -> 14.8 us  [from_everyone(): return lax.all_to_all(copies, axis, split_axis=0, concat_axis=0, tiled=True)]
  transfers between devices with their start and end apart: 8 -> 8, of which waited for: 7 -> 6; matrix products, arithmetic and copies ran while one was open for 4% -> 5% of each run, Pallas kernels for 0% -> 0%
where the time goes in v1:
time: 604 us; the launch traced here: 603 us
  waiting for transfers between devices  386 us (64%)
  starting transfers between devices  108 us (18%)
  blocking collectives  47.5 us (8%)
  local copies, waits for them, and re-layouts  25.5 us (4%)
  between operations  13.7 us (2%)
  other arithmetic  10.9 us (2%)
  matrix products  10.7 us (2%)
    all_gather x2, waiting for transfers between devices, sent_together(): lax.all_gather(both, axis, axis=dim, tiled=True)  343 us
    all_to_all x3, starting transfers between devices, from_everyone(): return lax.all_to_all(copies, axis, split_axis=0, concat_axis=0, tiled=True)  75.2 us
    all_gather x1, blocking collectives, shards(): out_full = lax.all_gather(out_weight, 'fs', axis=1, tiled=True)  47.5 us
    all_to_all x2, waiting for transfers between devices, summed_on_arrival(): lax.all_to_all(blocks, axis, split_axis=0, concat_axis=0, tiled=True)  28.7 us
    unnamed x55, local copies, waits for them, and re-layouts  21.6 us
    all_to_all x2, starting transfers between devices, summed_on_arrival(): lax.all_to_all(blocks, axis, split_axis=0, concat_axis=0, tiled=True)  20 us
    all_to_all x3, waiting for transfers between devices, from_everyone(): return lax.all_to_all(copies, axis, split_axis=0, concat_axis=0, tiled=True)  14.8 us
    all_to_all x1, starting transfers between devices, shards(): down_full = lax.all_to_all(copies_2, 'fs', 1, 1, tiled=True)  13.1 us
  transfers between devices with their start and end apart: 8, of which 6 were waited for; matrix products, arithmetic and copies ran while one was open for 5% of the time, Pallas kernels for 0%

profile of v1, /device:TPU:33, one launch (start us, length us, event | category | flops | bytes accessed | tf_op | source)
XLA Modules:
  0.0 602.9 jit_solution(9841033654518660183)
XLA Ops:
  6.6 1.4 pad_maximum_fusion.1
  8.0 0.7 convert_element_type.85
  8.7 1.1 fusion.33
  9.8 1.0 fusion.35
  10.8 1.2 broadcast_in_dim.6
  12.0 44.9 %all-to-all-start = ((bf16[8,40,2048]{2,1,0:T(8,128)(2,1)}), bf16[8,40,2048]{2,1,0:T(8,128)(2,1)S(1)}, u32[]{:S(2)}, u32[]{:S(2)}) async-start(bf16[8,40,2048]{2,1,0:T(8,128)(2,1)} %broadcast_in_dim.6), calls=%async_computation | async-start | bytes 2621440 | tf_op jit(solution)/shard_map/all_to_all | solution.py:13
  56.9 0.6 constant_dynamic-update-slice_fusion.31
  57.6 0.6 constant_dynamic-update-slice_fusion.30
  58.2 0.6 constant_dynamic-update-slice_fusion.29
  58.9 0.6 constant_dynamic-update-slice_fusion.28
  59.5 0.7 constant_dynamic-update-slice_fusion.27
  60.2 0.6 constant_dynamic-update-slice_fusion.26
  60.8 0.6 constant_dynamic-update-slice_fusion.25
  61.4 0.7 dynamic-slice_convert_fusion
  62.1 0.6 constant_dynamic-update-slice_fusion.24
  62.8 0.6 constant_dynamic-update-slice_fusion.23
  63.4 0.6 constant_dynamic-update-slice_fusion.22
  64.1 47.5 %all_gather.10 = bf16[128,2048]{0,1:T(8,128)(2,1)S(1)} all-gather(bf16[128,64]{0,1:T(8,128)(2,1)S(1)} %copy-done.7), channel_id=1, replica_groups=mesh['grp'=2,'fs'=32,'tp'=8] {'fs'}, dimensions={1}, use_global_device_ids=true | all-gather | bytes 540672 | tf_op jit(solution)/shard_map/all_gather | solution.py:122
  111.6 37.2 %all-gather.3.cloned.1.call-done = bf16[2048,256]{1,0:T(8,128)(2,1)} async-done(((bf16[64,256]{1,0:T(8,128)(2,1)}), bf16[2048,256]{1,0:T(8,128)(2,1)}) %all-gather.3.cloned.1.call-update) | async-done | bytes 1048592 | tf_op jit(solution)/shard_map/all_gather | solution.py:33
  148.7 1.6 fusion.12
  151.0 0.6 fusion.103
  152.5 25.9 %all-to-all-start.1 = ((f32[8,1,640]{2,1,0:T(1,128)}), f32[8,1,640]{2,1,0:T(1,128)S(1)}, u32[]{:S(2)}, u32[]{:S(2)}) async-start(f32[8,1,640]{2,1,0:T(1,128)} %broadcast_in_dim.7), calls=%async_computation.1 | async-start | bytes 40960 | tf_op jit(solution)/shard_map/all_to_all | solution.py:13
  178.3 0.8 dynamic-slice_convert_fusion.3
  179.1 3.9 all-to-all-done.1
  183.3 1.6 convolution_convert_fusion
  184.9 4.3 all-to-all-start.2
  189.2 0.7 constant_dynamic-update-slice_fusion.21
  189.9 0.6 constant_dynamic-update-slice_fusion.20
  190.5 0.6 constant_dynamic-update-slice_fusion.19
  191.1 0.6 constant_dynamic-update-slice_fusion.18
  191.8 0.6 constant_dynamic-update-slice_fusion.17
  192.4 0.6 constant_dynamic-update-slice_fusion.16
  193.0 0.6 constant_dynamic-update-slice_fusion.15
  193.7 0.6 constant_dynamic-update-slice_fusion.14
  194.3 0.6 constant_dynamic-update-slice_fusion.13
  195.0 0.6 constant_dynamic-update-slice_fusion.12
  195.6 0.6 constant_dynamic-update-slice_fusion.11
  196.2 10.8 %all-to-all-done.2 = bf16[8,40,2048]{2,1,0:T(8,128)(2,1)S(1)} async-done(((bf16[8,40,2048]{2,1,0:T(8,128)(2,1)}), bf16[8,40,2048]{2,1,0:T(8,128)(2,1)S(1)}, u32[]{:S(2)}, u32[]{:S(2)}) %all-to-all-start.2) | async-done | bytes 1310752 | tf_op jit(solution)/shard_map/all_to_all | solution.py:56
  207.8 1.2 broadcast_in_dim.8
  209.0 4.4 all-to-all-start.3
  213.4 0.6 constant_dynamic-update-slice_fusion.10
  214.1 0.6 constant_dynamic-update-slice_fusion.9
  214.7 0.6 constant_dynamic-update-slice_fusion.8
  215.3 0.6 constant_dynamic-update-slice_fusion.7
  216.0 0.6 constant_dynamic-update-slice_fusion.6
  216.6 0.6 constant_dynamic-update-slice_fusion.5
  217.3 0.6 constant_dynamic-update-slice_fusion.4
  217.9 0.6 constant_dynamic-update-slice_fusion.3
  218.5 0.6 constant_dynamic-update-slice_fusion.2
  219.2 0.6 constant_dynamic-update-slice_fusion.1
  219.8 0.6 constant_dynamic-update-slice_fusion
  220.4 10.9 %all-to-all-done.3 = bf16[8,40,2048]{2,1,0:T(8,128)(2,1)S(1)} async-done(((bf16[8,40,2048]{2,1,0:T(8,128)(2,1)}), bf16[8,40,2048]{2,1,0:T(8,128)(2,1)S(1)}, u32[]{:S(2)}, u32[]{:S(2)}) %all-to-all-start.3) | async-done | bytes 1310752 | tf_op jit(solution)/shard_map/all_to_all | solution.py:13
  231.3 1.2 copy-done.2
  232.5 13.1 %all-to-all-start.4 = ((bf16[640,32,64]{0,2,1:T(8,128)(2,1)}), bf16[640,32,64]{0,2,1:T(8,128)(2,1)S(1)}, u32[]{:S(2)}, u32[]{:S(2)}) async-start(bf16[640,32,64]{0,2,1:T(8,128)(2,1)} %bitcast.42), calls=%async_computation.4 | async-start | bytes 5242880 | tf_op jit(solution)/shard_map/all_to_all | solution.py:142
  245.7 0.7 pad_maximum_fusion
  246.4 0.9 dynamic-slice_convert_fusion.2
  247.3 305.6 %all-gather.5.cloned.1.call-done = bf16[2048,1280]{1,0:T(8,128)(2,1)} async-done(((bf16[64,1280]{1,0:T(8,128)(2,1)}), bf16[2048,1280]{1,0:T(8,128)(2,1)}) %all-gather.5.cloned.1.call-update) | async-done | bytes 5242896 | tf_op jit(solution)/shard_map/all_gather | solution.py:33
  553.0 3.5 fusion.4
  557.0 1.2 fusion.7
  558.3 0.8 fusion.22
  559.1 2.3 convolution_convert_fusion.1
  561.4 15.6 %all-to-all-start.5 = ((bf16[8,40,2048]{2,1,0:T(8,128)(2,1)}), bf16[8,40,2048]{2,1,0:T(8,128)(2,1)S(1)}, u32[]{:S(2)}, u32[]{:S(2)}) async-start(bf16[8,40,2048]{2,1,0:T(8,128)(2,1)} %bitcast.96), calls=%async_computation.5 | async-start | bytes 2621440 | tf_op jit(solution)/shard_map/all_to_all | solution.py:56
  577.0 17.9 %all-to-all-done.5 = bf16[8,40,2048]{2,1,0:T(8,128)(2,1)S(1)} async-done(((bf16[8,40,2048]{2,1,0:T(8,128)(2,1)}), bf16[8,40,2048]{2,1,0:T(8,128)(2,1)S(1)}, u32[]{:S(2)}, u32[]{:S(2)}) %all-to-all-start.5) | async-done | bytes 1310752 | tf_op jit(solution)/shard_map/all_to_all | solution.py:56
  595.2 0.8 fusion.40
  (56 shorter events, 3.6 us)
Async XLA Ops:
  6.5 50.4 %copy-start = (bf16[640,64]{0,1:T(8,128)(2,1)S(1)}, bf16[640,64]{0,1:T(8,128)(2,1)}, u32[]{:S(2)}) copy-start(bf16[640,64]{0,1:T(8,128)(2,1)} %param.26) | copy-start | bytes 245764
  6.5 142.2 %all-gather.3.cloned.1.call-start = ((), (), s32[]{:S(2)}) async-start(), calls=%async_computation.6 | async-start | bytes 1081344 | tf_op jit(solution)/shard_map/all_gather | solution.py:33
  10.8 53.3 %copy-start.7 = (bf16[128,64]{0,1:T(8,128)(2,1)S(1)}, bf16[128,64]{0,1:T(8,128)(2,1)}, u32[]{:S(2)}) copy-start(bf16[128,64]{0,1:T(8,128)(2,1)} %param.20) | copy-start | bytes 49156
  12.0 99.5 %all-to-all-start = ((bf16[8,40,2048]{2,1,0:T(8,128)(2,1)}), bf16[8,40,2048]{2,1,0:T(8,128)(2,1)S(1)}, u32[]{:S(2)}, u32[]{:S(2)}) async-start(bf16[8,40,2048]{2,1,0:T(8,128)(2,1)} %broadcast_in_dim.6), calls=%async_computation | async-start | bytes 2621440 | tf_op jit(solution)/shard_map/all_to_all | solution.py:13
  148.7 1.7 copy-start.4
  151.6 38.3 %copy-start.8 = (bf16[2048]{0:T(1024)(128)(2,1)S(1)}, bf16[2048]{0:T(1024)(128)(2,1)}, u32[]{:S(2)}) copy-start(bf16[2048]{0:T(1024)(128)(2,1)} %param.21) | copy-start | bytes 12292
  151.6 38.2 %copy-start.9 = (bf16[2048]{0:T(1024)(128)(2,1)S(1)}, bf16[2048]{0:T(1024)(128)(2,1)}, u32[]{:S(2)}) copy-start(bf16[2048]{0:T(1024)(128)(2,1)} %param.22) | copy-start | bytes 12292
  152.5 30.5 %all-to-all-start.1 = ((f32[8,1,640]{2,1,0:T(1,128)}), f32[8,1,640]{2,1,0:T(1,128)S(1)}, u32[]{:S(2)}, u32[]{:S(2)}) async-start(f32[8,1,640]{2,1,0:T(1,128)} %broadcast_in_dim.7), calls=%async_computation.1 | async-start | bytes 40960 | tf_op jit(solution)/shard_map/all_to_all | solution.py:13
  184.9 22.5 %copy-start.1 = (bf16[40,2048]{1,0:T(8,128)(2,1)S(1)}, bf16[40,2048]{1,0:T(8,128)(2,1)}, u32[]{:S(2)}) copy-start(bf16[40,2048]{1,0:T(8,128)(2,1)} %param.14) | copy-start | bytes 491524
  184.9 22.2 %all-to-all-start.2 = ((bf16[8,40,2048]{2,1,0:T(8,128)(2,1)}), bf16[8,40,2048]{2,1,0:T(8,128)(2,1)S(1)}, u32[]{:S(2)}, u32[]{:S(2)}) async-start(bf16[8,40,2048]{2,1,0:T(8,128)(2,1)} %bitcast.35), calls=%async_computation.2 | async-start | bytes 2621440 | tf_op jit(solution)/shard_map/all_to_all | solution.py:56
  209.0 22.3 %all-to-all-start.3 = ((bf16[8,40,2048]{2,1,0:T(8,128)(2,1)}), bf16[8,40,2048]{2,1,0:T(8,128)(2,1)S(1)}, u32[]{:S(2)}, u32[]{:S(2)}) async-start(bf16[8,40,2048]{2,1,0:T(8,128)(2,1)} %broadcast_in_dim.8), calls=%async_computation.3 | async-start | bytes 2621440 | tf_op jit(solution)/shard_map/all_to_all | solution.py:13
  231.3 1.2 copy-start.2
  231.3 14.4 %copy-start.5 = (bf16[64,640]{1,0:T(8,128)(2,1)S(1)}, bf16[64,640]{1,0:T(8,128)(2,1)}, u32[]{:S(2)}) copy-start(bf16[64,640]{1,0:T(8,128)(2,1)} %param.24) | copy-start | bytes 245764
  231.3 14.4 %copy-start.6 = (bf16[64,640]{1,0:T(8,128)(2,1)S(1)}, bf16[64,640]{1,0:T(8,128)(2,1)}, u32[]{:S(2)}) copy-start(bf16[64,640]{1,0:T(8,128)(2,1)} %param.23) | copy-start | bytes 245764
  232.5 326.6 %all-to-all-start.4 = ((bf16[640,32,64]{0,2,1:T(8,128)(2,1)}), bf16[640,32,64]{0,2,1:T(8,128)(2,1)S(1)}, u32[]{:S(2)}, u32[]{:S(2)}) async-start(bf16[640,32,64]{0,2,1:T(8,128)(2,1)} %bitcast.42), calls=%async_computation.4 | async-start | bytes 5242880 | tf_op jit(solution)/shard_map/all_to_all | solution.py:142
  245.6 307.4 %all-gather.5.cloned.1.call-start = ((), (), s32[]{:S(2)}) async-start(), calls=%async_computation.7 | async-start | bytes 5406720 | tf_op jit(solution)/shard_map/all_gather | solution.py:33
  553.0 3.5 copy-start.3
  553.0 4.1 copy-start.11
  561.4 15.6 %copy-start.10 = (bf16[2048]{0:T(1024)(128)(2,1)S(1)}, bf16[2048]{0:T(1024)(128)(2,1)}, u32[]{:S(2)}) copy-start(bf16[2048]{0:T(1024)(128)(2,1)} %param.27) | copy-start | bytes 12292
  561.4 33.5 %all-to-all-start.5 = ((bf16[8,40,2048]{2,1,0:T(8,128)(2,1)}), bf16[8,40,2048]{2,1,0:T(8,128)(2,1)S(1)}, u32[]{:S(2)}, u32[]{:S(2)}) async-start(bf16[8,40,2048]{2,1,0:T(8,128)(2,1)} %bitcast.96), calls=%async_computation.5 | async-start | bytes 2621440 | tf_op jit(solution)/shard_map/all_to_all | solution.py:56
Sparse Core Ops, SparseCore 0:
  9.4 139.2 all-gather.2
  248.5 304.3 all-gather.4
